TPU v7x, 32 devices: a whole 2x2x4 slice. The times are simulated.
32 devices in a mesh: sp: 8 (over z, x), tp: 4 (over y, core).
Axes of the slice: x: 2, y: 2, z: 4, core: 2. Of those that a mesh axis runs over, the one named last changes fastest.
Arguments:
- query_a: bfloat16 [1024, 2048], P('sp', 'tp'), may hold values from -6 to 6
- key_a: bfloat16 [1024, 2048], P('sp', 'tp'), may hold values from -6 to 6
- value_a: bfloat16 [1024, 4096], P('sp', 'tp'), may hold values from -6 to 6
- query_b: bfloat16 [1024, 2048], P('sp', 'tp'), may hold values from -6 to 6
- key_b: bfloat16 [1024, 2048], P('sp', 'tp'), may hold values from -6 to 6
- value_b: bfloat16 [1024, 2048], P('sp', 'tp'), may hold values from -6 to 6
- in_gate: float32 [2, 2, 16, 1024], P(None, None, 'tp', 'sp'), may hold values from -6 to 300
- forget_gate: float32 [2, 2, 16, 1024], P(None, None, 'tp', 'sp'), may hold values from 0 to 14.1
- head_gain_a: float32 [16, 256], P('tp'), may hold values from 0.1 to 1.9
- head_gain_b: float32 [16, 128], P('tp'), may hold values from 0.1 to 1.9
- out_weight_a: bfloat16 [4096, 2048], P('tp'), may hold values from -0.078125 to 0.078125
- out_weight_b: bfloat16 [2048, 2048], P('tp'), may hold values from -0.078125 to 0.078125
- residual: bfloat16 [2048, 1024], P('tp', 'sp'), may hold values from -40 to 40
- norm_gain: float32 [2048], P('tp'), may hold values from 0.1 to 1.9
- routes: int32 [1024, 2], P('sp'), may hold values from 0 to 7, all different within a row; in each aligned block of 128 rows (0 to 127, 128 to 255, ...) at most 64 rows name the same one
- route_weights: float32 [1024, 2], P('sp'), may hold values from 0.2 to 1
- expert_gate: bfloat16 [8, 2048, 4096], P('sp', None, 'tp'), may hold values from -0.125 to 0.125
- expert_up: bfloat16 [8, 2048, 4096], P('sp', None, 'tp'), may hold values from -0.125 to 0.125
- expert_down: bfloat16 [8, 4096, 2048], P('sp', 'tp'), may hold values from -0.09375 to 0.09375
Outputs:
- layer_output: bfloat16 [2048, 1024], P('tp', 'sp')
Inputs may be any that keep to these rules, and one draw needn't show every extreme that they name: `routes`: each row names 2 different experts. In each aligned block of 128 rows (the rows of one index of sp) no expert is named by more than 64 rows, a bound that some blocks reach.
All inputs are finite; a program needn't handle non-finite values.
Results may differ from a plain program's by a relative error of at most 0.012.
Values may be sent and summed in bfloat16 or wider, within the bound.
No kernel may reach another device: no remote copies, remote signals or barrier semaphores. Data moves between devices by JAX's collectives and lax.ppermute only.
A program may use at most 128 MiB of HBM per device.

v0:
```python
import jax
import jax.numpy as jnp
from jax import lax
from jax.sharding import PartitionSpec as P

BLOCK = 128


EPSILON = 1e-06
LOG_FLOOR = -1e30
PRECISE = lax.Precision.HIGH


def carried_in(value, axis, join, neutral, backward):
    count, mine = (lax.axis_size(axis), lax.axis_index(axis))
    pieces = jax.tree.map(lambda part: lax.all_gather(part, axis), value)
    if backward:
        pieces = jax.tree.map(lambda part: part[::-1], pieces)
        mine = count - 1 - mine
    so_far = jax.tree.map(
        lambda part, zero: jnp.full_like(part, 0) + jnp.asarray(zero, part.dtype), value, neutral
    )

    def turn(position, so_far):
        longer = join(so_far, jax.tree.map(lambda part: part[position], pieces))
        return jax.tree.map(lambda new, old: jnp.where(position < mine, new, old), longer, so_far)

    return lax.fori_loop(0, count - 1, turn, so_far)


def heads_first(tensor, head_count):
    return tensor.reshape(tensor.shape[0], head_count, -1).transpose(1, 0, 2)


def block_pass(queries, keys_in, values_in, log_input, log_decay, start):
    head_count, length, width_k = queries.shape
    blocks = length // BLOCK
    q_scale = width_k ** (-0.5)
    lower_mask = jnp.tril(jnp.ones((BLOCK, BLOCK), dtype=bool))

    def to_blocks(tensor):
        return jnp.moveaxis(tensor.reshape(head_count, blocks, BLOCK, *tensor.shape[2:]), 1, 0)

    def block_step(carried_state, inputs_block):
        memory, normal, stabilizer = carried_state
        q_block, k_block, v_block, in_block, decay_block = inputs_block
        cumulative = jnp.cumsum(decay_block, axis=-1)
        running_log_decay = cumulative + stabilizer[:, None]
        log_weights = jnp.where(
            lower_mask,
            cumulative[:, :, None] - cumulative[:, None, :] + in_block[:, None, :],
            -jnp.inf,
        )
        row_peak = jnp.maximum(running_log_decay, jnp.max(log_weights, axis=-1))
        carried_weight = jnp.exp(running_log_decay - row_peak)
        products = (
            jnp.einsum("htd,hsd->hts", q_block, k_block, preferred_element_type=jnp.float32)
            * q_scale
        )
        scores = products * jnp.exp(log_weights - row_peak[:, :, None])
        q_float = q_block.astype(jnp.float32) * q_scale
        numerator = carried_weight[:, :, None] * jnp.einsum(
            "htd,hde->hte", q_float, memory, precision=PRECISE
        )
        numerator = numerator + jnp.einsum(
            "hts,hse->hte", scores.astype(jnp.bfloat16), v_block, preferred_element_type=jnp.float32
        )
        denominator = carried_weight * jnp.einsum(
            "htd,hd->ht", q_float, normal, precision=PRECISE
        ) + jnp.sum(scores, axis=-1)
        decay_total = cumulative[:, -1]
        tail_logs = decay_total[:, None] - cumulative + in_block
        new_stabilizer = jnp.maximum(decay_total + stabilizer, jnp.max(tail_logs, axis=-1))
        keep_scale = jnp.exp(decay_total + stabilizer - new_stabilizer)
        weighted_keys = (
            k_block.astype(jnp.float32) * jnp.exp(tail_logs - new_stabilizer[:, None])[:, :, None]
        )
        memory = keep_scale[:, None, None] * memory + jnp.einsum(
            "hsd,hse->hde", weighted_keys, v_block.astype(jnp.float32), precision=PRECISE
        )
        normal = keep_scale[:, None] * normal + jnp.sum(weighted_keys, axis=1)
        return ((memory, normal, new_stabilizer), (numerator, denominator, row_peak))

    blocked = tuple(
        (to_blocks(tensor) for tensor in (queries, keys_in, values_in, log_input, log_decay))
    )
    final_state, outputs = lax.scan(block_step, start, blocked)
    joined = [
        jnp.moveaxis(tensor, 0, 1).reshape(head_count, length, *tensor.shape[3:])
        for tensor in outputs
    ]
    return (final_state, joined[0], joined[1], joined[2])


def device_summary(view):
    queries, keys_in, values_in, log_input, log_decay = view
    cumulative = jnp.cumsum(log_decay, axis=-1)
    decay_total = cumulative[:, -1]
    tail_logs = decay_total[:, None] - cumulative + log_input
    stabilizer = jnp.max(tail_logs, axis=-1)
    weighted_keys = (
        keys_in.astype(jnp.float32) * jnp.exp(tail_logs - stabilizer[:, None])[:, :, None]
    )
    memory = jnp.einsum(
        "hsd,hse->hde", weighted_keys, values_in.astype(jnp.float32), precision=PRECISE
    )
    return (decay_total, memory, jnp.sum(weighted_keys, axis=1), stabilizer)


def merge_group(earlier, later):
    drop_early, memory_early, normal_early, top_early = earlier
    drop_late, memory_late, normal_late, top_late = later
    shifted = drop_late + top_early
    merged_top = jnp.maximum(shifted, top_late)
    scale_early = jnp.exp(shifted - merged_top)
    scale_late = jnp.exp(top_late - merged_top)
    memory = scale_early[:, None, None] * memory_early + scale_late[:, None, None] * memory_late
    normal = scale_early[:, None] * normal_early + scale_late[:, None] * normal_late
    return (drop_early + drop_late, memory, normal, merged_top)


def join_states(earlier, later):
    return merge_group(earlier[:4], later[:4]) + merge_group(earlier[4:], later[4:])


def pass_states(pieces, backward):
    identity = tuple(
        (
            jnp.full_like(piece, LOG_FLOOR) if position % 4 == 3 else jnp.zeros_like(piece)
            for position, piece in enumerate(pieces)
        )
    )
    if backward:
        return carried_in(pieces, "sp", join_states, identity, True)
    return carried_in(pieces, "sp", join_states, identity, False)


def normalize(numerator, denominator, row_peak):
    return numerator / jnp.maximum(jnp.abs(denominator), jnp.exp(-row_peak))[:, :, None]


def direction_outputs(views, backward):
    finished = []
    pieces = ()
    for view in views:
        pieces = pieces + device_summary(view)
    incoming = pass_states(pieces, backward)
    for number in range(2):
        outcome = block_pass(*views[number], incoming[4 * number + 1 : 4 * number + 4])
        finished.append(normalize(outcome[1], outcome[2], outcome[3]))
    return finished


def local(
    query_a,
    key_a,
    value_a,
    query_b,
    key_b,
    value_b,
    in_gate,
    forget_gate,
    head_gain_a,
    head_gain_b,
    out_weight_a,
    out_weight_b,
    residual,
    norm_gain,
    routes,
    route_weights,
    expert_gate,
    expert_up,
    expert_down,
):
    head_count = head_gain_a.shape[0]
    log_decay = jax.nn.log_sigmoid(forget_gate)
    groups = (
        (
            heads_first(query_a, head_count),
            heads_first(key_a, head_count),
            heads_first(value_a, head_count),
        ),
        (
            heads_first(query_b, head_count),
            heads_first(key_b, head_count),
            heads_first(value_b, head_count),
        ),
    )
    results = []
    for direction in range(2):
        views = []
        for group_index in range(2):
            tensors = groups[group_index] + (
                in_gate[direction, group_index],
                log_decay[direction, group_index],
            )
            if direction == 1:
                tensors = tuple((jnp.flip(tensor, 1) for tensor in tensors))
            views.append(tensors)
        results.append(direction_outputs(views, direction == 1))
    normed_heads = []
    for group_index, head_gain in enumerate((head_gain_a, head_gain_b)):
        both = results[0][group_index] + jnp.flip(results[1][group_index], 1)
        scaled = (
            both
            * lax.rsqrt(jnp.mean(both * both, axis=-1, keepdims=True) + EPSILON)
            * head_gain[:, None, :]
        )
        normed_heads.append(scaled.astype(jnp.bfloat16))
    heads_a, heads_b = normed_heads
    weights_a = out_weight_a.reshape(head_count, -1, out_weight_a.shape[1])
    weights_b = out_weight_b.reshape(head_count, -1, out_weight_b.shape[1])
    first_term = jnp.einsum("hse,hec->cs", heads_a, weights_a, preferred_element_type=jnp.float32)
    mix = lax.psum_scatter(
        (
            first_term
            + jnp.einsum("hse,hec->cs", heads_b, weights_b, preferred_element_type=jnp.float32)
        ).astype(jnp.bfloat16),
        "tp",
        scatter_dimension=0,
        tiled=True,
    ).astype(jnp.float32)
    updated = residual.astype(jnp.float32) + mix
    squares = lax.psum(jnp.sum(updated * updated, axis=0), "tp")
    whole_width = residual.shape[0] * lax.axis_size("tp")
    normed = (
        updated * lax.rsqrt(squares / whole_width + EPSILON)[None, :] * norm_gain[:, None]
    ).astype(jnp.bfloat16)
    token_count = routes.shape[0]
    top_count = routes.shape[1]
    expert_count = lax.axis_size("sp") * expert_gate.shape[0]
    slot_count = 2 * token_count * top_count // expert_count
    flat_routes = routes.reshape(-1)
    hits = (flat_routes[:, None] == jnp.arange(expert_count, dtype=jnp.int32)[None, :]).astype(
        jnp.int32
    )
    ranks = jnp.sum((jnp.cumsum(hits, axis=0) - 1) * hits, axis=1)
    targets = (flat_routes * slot_count + ranks).reshape(token_count, top_count)
    slot_ids = jnp.arange(expert_count * slot_count, dtype=jnp.int32)[:, None]
    selectors = [
        (slot_ids == targets[None, :, ordering_index]).astype(jnp.bfloat16)
        for ordering_index in range(top_count)
    ]
    dispatch = selectors[0]
    ordering_index = 1
    dispatch = dispatch + selectors[ordering_index]
    buffer = jnp.einsum("ps,ds->pd", dispatch, normed, preferred_element_type=jnp.float32)
    buffer = buffer.astype(jnp.bfloat16).reshape(expert_count, slot_count, -1)
    arrived = lax.all_to_all(buffer, "sp", split_axis=0, concat_axis=0, tiled=True)
    piece = lax.all_gather(arrived, "tp", axis=2, tiled=True)
    flat_rows = piece.reshape(-1, piece.shape[-1])
    gate_rows = expert_gate[0]
    up_rows = expert_up[0]
    gate = jnp.dot(flat_rows, gate_rows, preferred_element_type=jnp.float32)
    upward = jnp.dot(flat_rows, up_rows, preferred_element_type=jnp.float32)
    hidden = (
        (jax.nn.silu(gate) * upward)
        .astype(jnp.bfloat16)
        .reshape(arrived.shape[0], arrived.shape[1], -1)
    )
    sources = hidden.shape[0]
    hidden_rows = hidden.reshape(-1, hidden.shape[-1])
    columns = expert_down[0]
    summed = lax.psum_scatter(
        jnp.einsum("rf,fc->cr", hidden_rows, columns, preferred_element_type=jnp.float32).astype(
            jnp.bfloat16
        ),
        "tp",
        scatter_dimension=0,
        tiled=True,
    ).astype(jnp.float32)
    outgoing = summed.astype(jnp.bfloat16).reshape(summed.shape[0], sources, slot_count)
    returned = lax.all_to_all(outgoing, "sp", split_axis=1, concat_axis=1, tiled=True)
    returned = returned.reshape(returned.shape[0], -1)
    combined = updated
    for ordering_index in range(top_count):
        picked = jnp.dot(returned, selectors[ordering_index], preferred_element_type=jnp.float32)
        combined = combined + route_weights[:, ordering_index][None, :] * picked
    return combined.astype(jnp.bfloat16)


def solution(mesh):
    placed = (
        P("sp", "tp"),
        P("sp", "tp"),
        P("sp", "tp"),
        P("sp", "tp"),
        P("sp", "tp"),
        P("sp", "tp"),
        P(None, None, "tp", "sp"),
        P(None, None, "tp", "sp"),
        P("tp", None),
        P("tp", None),
        P("tp", None),
        P("tp", None),
        P("tp", "sp"),
        P("tp"),
        P("sp", None),
        P("sp", None),
        P("sp", None, "tp"),
        P("sp", None, "tp"),
        P("sp", "tp", None),
    )
    return jax.shard_map(
        local, mesh=mesh, in_specs=placed, out_specs=P("tp", "sp"), check_vma=False
    )
```

profile of v0, /device:TPU:0, one launch (start us, length us, event | category | flops | bytes accessed | tf_op | source)
XLA Modules:
  0.0 495.7 jit_solution(4652735712022758953)
XLA Ops:
  46.2 24.2 %all-reduce.8 = (f32[32]{0:T(128)}, f32[32]{0:T(128)}, f32[32]{0:T(128)}, f32[32]{0:T(128)}, f32[32]{0:T(128)}, /*index=5*/f32[32]{0:T(128)}, f32[32]{0:T(128)}, f32[32]{0:T(128)}) all-reduce(f32[32]{0:T(128)} %dynamic-update-slice.4, f32[32]{0:T(128)} %dynamic-update-slice.5, ...), channel_id=10, replica_groups=mesh['sp'=8,'tp'=4] {'sp'}, use_global_device_ids=true, to_apply=%add.4 | all-reduce | flops 256 | bytes 2048
  75.6 27.6 %all-gather.18 = f32[8,4,128]{2,1,0:T(4,128)} all-gather(f32[1,4,128]{2,1,0:T(4,128)} %bitcast.399), channel_id=13, replica_groups=mesh['sp'=8,'tp'=4] {'sp'}, dimensions={0}, use_global_device_ids=true | all-gather | bytes 18432 | tf_op jit(solution)/shard_map/all_gather | solution.py:16
  109.6 28.0 %all-gather.19 = f32[8,4,128]{2,1,0:T(4,128)} all-gather(f32[1,4,128]{2,1,0:T(4,128)} %bitcast.397), channel_id=17, replica_groups=mesh['sp'=8,'tp'=4] {'sp'}, dimensions={0}, use_global_device_ids=true | all-gather | bytes 18432 | tf_op jit(solution)/shard_map/all_gather | solution.py:16
  140.6 2.9 rev.81
  146.2 27.1 %all-gather.16 = f32[8,4,128]{2,1,0:T(4,128)} all-gather(f32[1,4,128]{2,1,0:T(4,128)} %bitcast.398), channel_id=5, replica_groups=mesh['sp'=8,'tp'=4] {'sp'}, dimensions={0}, use_global_device_ids=true | all-gather | bytes 18432 | tf_op jit(solution)/shard_map/all_gather | solution.py:16
  175.9 27.5 %all-gather.17 = f32[8,4,128]{2,1,0:T(4,128)} all-gather(f32[1,4,128]{2,1,0:T(4,128)} %bitcast.396), channel_id=9, replica_groups=mesh['sp'=8,'tp'=4] {'sp'}, dimensions={0}, use_global_device_ids=true | all-gather | bytes 18432 | tf_op jit(solution)/shard_map/all_gather | solution.py:16
  205.1 2.9 rev.83
  208.0 2.0 fusion.65
  209.9 3.1 rev.79
  213.1 4.6 rev.71
  217.7 58.3 %while.11 = (s32[]{:T(128)}, f32[4,128,256]{2,1,0:T(8,128)S(1)}, f32[4,128]{1,0:T(4,128)}, f32[4]{0:T(128)}, f32[4,128,128]{2,1,0:T(8,128)}, /*index=5*/f32[4,12...) while((s32[]{:T(128)}, f32[4,128,256]{2,1,0:T(8,128)S(1)}, ...), condition=%wide.region_17.18_spmd.clone, body=%wide.region_16.17_spmd.clone.sunk | while | flops 988220 | bytes 2372229 | solution.py:28
  281.5 2.6 rev.82
  284.2 52.5 %while.10 = (s32[]{:T(128)}, f32[4,128,256]{2,1,0:T(8,128)S(1)}, f32[4,128]{1,0:T(4,128)S(1)}, f32[4]{0:T(128)}, f32[4,128,128]{2,1,0:T(8,128)S(1)}, /*index=5*/...) while((s32[]{:T(128)}, f32[4,128,256]{2,1,0:T(8,128)S(1)}, ...), condition=%wide.region_7.8_spmd.clone, body=%wide.region_6.7_spmd.clone.sunk | while | flops 988220 | bytes 2372229 | solution.py:28
  341.6 1.9 rev.84
  347.0 3.0 convolution_bitcast_fusion
  353.1 17.4 %reduce-scatter.3.cloned.1.call-done = bf16[512,128]{0,1:T(8,128)(2,1)} async-done(((bf16[2048,128]{0,1:T(8,128)(2,1)}), bf16[512,128]{0,1:T(8,128)(2,1)}) %reduce-scatter.3.cloned.1.call-update) | async-done | bytes 131088 | tf_op jit(solution)/shard_map/reduce_scatter | solution.py:214
  371.6 5.8 %psum.7 = f32[128]{0:T(128)S(1)} all-reduce(f32[128]{0:T(128)S(1)} %multiply_reduce_fusion.1), channel_id=1, replica_groups=mesh['sp'=8,'tp'=4] {'tp'}, use_global_device_ids=true, to_apply=%region_31.32 | all-reduce | flops 128 | bytes 1024 | tf_op jit(solution)/shard_map/psum | solution.py:224
  378.6 19.8 %all_to_all.10 = bf16[8,64,512]{2,1,0:T(8,128)(2,1)} all-to-all(bf16[8,64,512]{2,1,0:T(8,128)(2,1)S(1)} %bitcast.376), channel_id=1, replica_groups=mesh['sp'=8,'tp'=4] {'sp'}, dimensions={0} | all-to-all | bytes 1048576 | tf_op jit(solution)/shard_map/all_to_all | solution.py:249
  398.7 20.6 %all-gather.26.cloned.1.call-done = bf16[8,64,2048]{2,1,0:T(8,128)(2,1)} async-done(((bf16[8,64,512]{2,1,0:T(8,128)(2,1)}), bf16[8,64,2048]{2,1,0:T(8,128)(2,1)}) %all-gather.26.cloned.1.call-update) | async-done | bytes 2097168 | tf_op jit(solution)/shard_map/all_gather | solution.py:250
  419.3 6.5 %fusion.32 = f32[512,1024]{1,0:T(8,128)} fusion(bf16[512,2048]{1,0:T(8,128)(2,1)} %bitcast.404, bf16[1,2048,1024]{2,1,0:T(8,128)(2,1)} %param.39), kind=kOutput, calls=%fused_computation.64 | convolution fusion | flops 2147483648 | bytes 8388608 | tf_op jit(solution)/shard_map/dot_general | solution.py:254
  425.8 10.5 %fusion.37 = bf16[2048,512]{0,1:T(8,128)(2,1)} fusion(bf16[1,1024,2048]{2,1,0:T(8,128)(2,1)} %param.41, f32[512,1024]{1,0:T(8,128)} %fusion.32, bf16[512,2048]{1,0:T(8,128)(2,1)} %bitcast.405, bf16[1,2048,1024]{2,1,0:T(8,128)(2,1)} %param.40), kind=kOutput, calls=%fused_computation.67 | convolution fusion | flops 4299161600 | bytes 14680064 | tf_op jit(solution)/shard_map/rf,fc->cr/dot_general | solution.py:265
  436.4 31.3 %reduce-scatter.5.cloned.1.call-done = bf16[512,512]{0,1:T(8,128)(2,1)} async-done(((bf16[2048,512]{0,1:T(8,128)(2,1)}), bf16[512,512]{0,1:T(8,128)(2,1)}) %reduce-scatter.5.cloned.1.call-update) | async-done | bytes 524304 | tf_op jit(solution)/shard_map/reduce_scatter | solution.py:264
  467.7 5.5 %all-to-all-start.1 = ((bf16[512,8,64]{0,2,1:T(8,128)(2,1)}), bf16[512,8,64]{0,2,1:T(8,128)(2,1)S(1)}, u32[]{:S(2)}, u32[]{:S(2)}) async-start(bf16[512,8,64]{0,2,1:T(8,128)(2,1)} %bitcast.391), calls=%async_computation.3 | async-start | bytes 1048576 | tf_op jit(solution)/shard_map/all_to_all | solution.py:273
  473.2 14.3 %all-to-all-done.1 = bf16[512,8,64]{0,2,1:T(8,128)(2,1)S(1)} async-done(((bf16[512,8,64]{0,2,1:T(8,128)(2,1)}), bf16[512,8,64]{0,2,1:T(8,128)(2,1)S(1)}, u32[]{:S(2)}, u32[]{:S(2)}) %all-to-all-start.1) | async-done | bytes 524320 | tf_op jit(solution)/shard_map/all_to_all | solution.py:273
  (346 shorter events, 191.3 us)
Async XLA Ops:
  6.5 343.4 %copy-start = (bf16[512,2048]{1,0:T(8,128)(2,1)S(1)}, bf16[512,2048]{1,0:T(8,128)(2,1)}, u32[]{:S(2)}) copy-start(bf16[512,2048]{1,0:T(8,128)(2,1)} %param.34) | copy-start | bytes 6291460
  6.5 7.4 %copy-start.11 = (bf16[128,1024]{1,0:T(8,128)(2,1)S(1)}, bf16[128,1024]{1,0:T(8,128)(2,1)}, u32[]{:S(2)}) copy-start(bf16[128,1024]{1,0:T(8,128)(2,1)} %param.25) | copy-start | bytes 786436
  6.5 7.8 %copy-start.2 = (bf16[128,512]{1,0:T(8,128)(2,1)S(1)}, bf16[128,512]{1,0:T(8,128)(2,1)}, u32[]{:S(2)}) copy-start(bf16[128,512]{1,0:T(8,128)(2,1)} %param.24) | copy-start | bytes 393220
  6.5 203.4 %all-gather.34.cloned.1.call-start = ((), (), s32[]{:S(2)}) async-start(), calls=%async_computation.10 | async-start | bytes 2359296 | tf_op jit(solution)/shard_map/all_gather | solution.py:16
  12.1 8.5 %copy-start.7 = (bf16[128,512]{1,0:T(8,128)(2,1)S(1)}, bf16[128,512]{1,0:T(8,128)(2,1)}, u32[]{:S(2)}) copy-start(bf16[128,512]{1,0:T(8,128)(2,1)} %param.27) | copy-start | bytes 393220
  12.1 8.5 %copy-start.17 = (bf16[128,512]{1,0:T(8,128)(2,1)S(1)}, bf16[128,512]{1,0:T(8,128)(2,1)}, u32[]{:S(2)}) copy-start(bf16[128,512]{1,0:T(8,128)(2,1)} %param.28) | copy-start | bytes 393220
  12.3 12.4 %copy-start.9 = (bf16[4,128,128]{2,1,0:T(8,128)(2,1)}, bf16[4,128,128]{2,1,0:T(8,128)(2,1)S(1)}, u32[]{:S(2)}) copy-start(bf16[4,128,128]{2,1,0:T(8,128)(2,1)S(1)} %rev.77) | copy-start | bytes 393220
  13.7 199.3 %all-gather.32.cloned.1.call-start = ((), (), s32[]{:S(2)}) async-start(), calls=%async_computation.9 | async-start | bytes 4718592 | tf_op jit(solution)/shard_map/all_gather | solution.py:16
  14.4 8.7 %copy-start.13 = (bf16[4,128,256]{2,1,0:T(8,128)(2,1)}, bf16[4,128,256]{2,1,0:T(8,128)(2,1)S(1)}, u32[]{:S(2)}) copy-start(bf16[4,128,256]{2,1,0:T(8,128)(2,1)S(1)} %rev.70) | copy-start | bytes 786436
  14.6 12.1 %copy-start.4 = (bf16[4,128,128]{2,1,0:T(8,128)(2,1)}, bf16[4,128,128]{2,1,0:T(8,128)(2,1)S(1)}, u32[]{:S(2)}) copy-start(bf16[4,128,128]{2,1,0:T(8,128)(2,1)S(1)} %rev.69) | copy-start | bytes 393220
  16.7 267.5 %all-gather.30.cloned.1.call-start = ((), (), s32[]{:S(2)}) async-start(), calls=%async_computation.8 | async-start | bytes 2359296 | tf_op jit(solution)/shard_map/all_gather | solution.py:16
  21.8 262.3 %all-gather.28.cloned.1.call-start = ((), (), s32[]{:S(2)}) async-start(), calls=%async_computation.7 | async-start | bytes 4718592 | tf_op jit(solution)/shard_map/all_gather | solution.py:16
  23.2 347.4 %reduce-scatter.3.cloned.1.call-start = ((), (), s32[]{:S(2)}) async-start(), calls=%async_computation.4 | async-start | bytes 655360 | tf_op jit(solution)/shard_map/reduce_scatter | solution.py:214
  284.2 52.5 %copy-start.36 = (f32[4,128]{1,0:T(4,128)S(1)}, f32[4,128]{1,0:T(4,128)}, u32[]{:S(2)}) copy-start(f32[4,128]{1,0:T(4,128)} %get-tuple-element.806) | copy-start | bytes 6148
  284.2 53.3 %copy-start.5 = (bf16[128,512]{0,1:T(8,128)(2,1)S(1)}, bf16[128,512]{0,1:T(8,128)(2,1)}, u32[]{:S(2)}) copy-start(bf16[128,512]{0,1:T(8,128)(2,1)} %copy.163) | copy-start | bytes 393220
  284.2 53.3 %copy-start.23 = (pred[128,128]{0,1:T(8,128)(4,1)S(1)}, pred[128,128]{0,1:T(8,128)(4,1)}, u32[]{:S(2)}) copy-start(pred[128,128]{0,1:T(8,128)(4,1)} %iota_compare_fusion.4) | copy-start | bytes 49156
  284.2 53.3 %copy-start.37 = (f32[4,128]{1,0:T(4,128)S(1)}, f32[4,128]{1,0:T(4,128)}, u32[]{:S(2)}) copy-start(f32[4,128]{1,0:T(4,128)} %get-tuple-element.911) | copy-start | bytes 6148
  340.0 6.7 %copy-start.18 = (bf16[128,512]{1,0:T(8,128)(2,1)S(1)}, bf16[128,512]{1,0:T(8,128)(2,1)}, u32[]{:S(2)}) copy-start(bf16[128,512]{1,0:T(8,128)(2,1)} %param.28) | copy-start | bytes 393220
  350.0 27.4 %copy-start.44 = (f32[512]{0:T(512)S(1)}, f32[512]{0:T(512)}, u32[]{:S(2)}) copy-start(f32[512]{0:T(512)} %param.36) | copy-start | bytes 6148
  351.4 68.0 %all-gather.26.cloned.1.call-start = ((), (), s32[]{:S(2)}) async-start(), calls=%async_computation.5 | async-start | bytes 2621440 | tf_op jit(solution)/shard_map/all_gather | solution.py:250
  398.5 69.2 %reduce-scatter.5.cloned.1.call-start = ((), (), s32[]{:S(2)}) async-start(), calls=%async_computation.6 | async-start | bytes 2621440 | tf_op jit(solution)/shard_map/reduce_scatter | solution.py:264
  436.4 36.9 %copy-start.49 = (f32[128,2]{0,1:T(2,128)S(1)}, f32[128,2]{0,1:T(2,128)}, u32[]{:S(2)}) copy-start(f32[128,2]{0,1:T(2,128)} %param.38) | copy-start | bytes 3076
  436.4 51.2 %copy-start.6 = (bf16[512,128]{0,1:T(8,128)(2,1)S(1)}, bf16[512,128]{0,1:T(8,128)(2,1)}, u32[]{:S(2)}) copy-start(bf16[512,128]{0,1:T(8,128)(2,1)} %reduce-scatter.3.cloned.1.call-done) | copy-start | bytes 393220
  467.7 19.8 %all-to-all-start.1 = ((bf16[512,8,64]{0,2,1:T(8,128)(2,1)}), bf16[512,8,64]{0,2,1:T(8,128)(2,1)S(1)}, u32[]{:S(2)}, u32[]{:S(2)}) async-start(bf16[512,8,64]{0,2,1:T(8,128)(2,1)} %bitcast.391), calls=%async_computation.3 | async-start | bytes 1048576 | tf_op jit(solution)/shard_map/all_to_all | solution.py:273
  (34 other events, 104.0 us)
Sparse Core Ops, SparseCore 0:
  13.9 52.1 all-gather.33
  68.2 71.7 all-gather.31
  142.2 48.0 all-gather.29
  192.3 71.3 all-gather.27
  351.5 19.0 reduce-scatter.2
  398.6 20.7 all-gather.25
  436.5 31.1 reduce-scatter.4
where the time goes:
time: 501 us; the launch traced here: 496 us
  blocking collectives  160 us (32%)
  other arithmetic  131 us (26%)
  waiting for transfers between devices  83.8 us (17%)
  local copies, waits for them, and re-layouts  63 us (13%)
  matrix products  36.8 us (7%)
  between operations  15 us (3%)
  starting transfers between devices  5.98 us (1%)
    all_gather x4, blocking collectives, carried_in(): pieces = jax.tree.map(lambda part: lax.all_gather(part, axis), value)  110 us
    select_n x70, other arithmetic, turn(): jnp.where(position < mine, new, old)  91.2 us
    reduce_scatter x1, waiting for transfers between devices, local(): lax.psum_scatter(jnp.einsum('rf,fc->cr', hidden_rows, columns, preferred_...  31.3 us
    unnamed x1, blocking collectives  24.2 us
    all_gather x1, waiting for transfers between devices, local(): piece = lax.all_gather(arrived, 'tp', axis=2, tiled=True)  20.6 us
    all_to_all x1, blocking collectives, local(): lax.all_to_all(buffer, 'sp', split_axis=0, concat_axis=0, tiled=True)  19.8 us
    unnamed x121, local copies, waits for them, and re-layouts  19.5 us
    exp x28, other arithmetic, merge_group(): scale_early = jnp.exp(shifted - merged_top)  19.3 us
  transfers between devices with their start and end apart: 8, of which 4 were waited for; matrix products, arithmetic and copies ran while one was open for 27% of the time, Pallas kernels for 0%

commit v1 on v0

v1 whole, which is shorter than its diff:
```python
import jax
import jax.numpy as jnp
from jax import lax
from jax.experimental import pallas as pl
from jax.experimental.pallas import tpu as pltpu
from jax.sharding import PartitionSpec as P

EPSILON = 1e-06
MASKED = -1e30
HIGHEST = lax.Precision.HIGHEST


def heads_kernel(offset, queries, keys_in, values_in, source_logs, target_logs, gain, heads):
    length, width_k = queries.shape
    products = lax.dot_general(
        queries[...], keys_in[...], (((1,), (1,)), ((), ())), preferred_element_type=jnp.float32
    ) * (width_k ** (-0.5))
    target = lax.broadcasted_iota(jnp.int32, products.shape, 0) + offset[0]
    source = lax.broadcasted_iota(jnp.int32, products.shape, 1)
    weights = None
    for direction in range(2):
        reached = source <= target if direction == 0 else source >= target
        logs = jnp.where(reached, source_logs[0, direction : direction + 1, :], MASKED)
        peak = jnp.max(logs, axis=1, keepdims=True)
        scores = products * jnp.exp(logs - peak)
        denominator = jnp.sum(scores, axis=1, keepdims=True)
        floor = jnp.exp(-(target_logs[0, :, direction : direction + 1] + peak))
        scaled = scores * (1.0 / jnp.maximum(jnp.abs(denominator), floor))
        weights = scaled if weights is None else weights + scaled
    both = jnp.dot(
        weights.astype(jnp.bfloat16), values_in[...], preferred_element_type=jnp.float32
    )
    spread = lax.rsqrt(jnp.mean(both * both, axis=1, keepdims=True) + EPSILON)
    heads[...] = (both * spread * gain[0]).astype(jnp.bfloat16)


def group_heads(offset, queries, keys_in, values_in, source_logs, target_logs, gain):
    head_count = gain.shape[0]
    length, total = queries.shape[0], keys_in.shape[0]
    width_k, width_v = queries.shape[1] // head_count, gain.shape[1]
    return pl.pallas_call(
        heads_kernel,
        grid_spec=pltpu.PrefetchScalarGridSpec(
            num_scalar_prefetch=1,
            grid=(head_count,),
            in_specs=[
                pl.BlockSpec((length, width_k), lambda h, o: (0, h)),
                pl.BlockSpec((total, width_k), lambda h, o: (0, h)),
                pl.BlockSpec((total, width_v), lambda h, o: (0, h)),
                pl.BlockSpec((1, 2, total), lambda h, o: (h, 0, 0)),
                pl.BlockSpec((1, length, 2), lambda h, o: (h, 0, 0)),
                pl.BlockSpec((1, 1, width_v), lambda h, o: (h, 0, 0)),
            ],
            out_specs=pl.BlockSpec((length, width_v), lambda h, o: (0, h)),
        ),
        out_shape=jax.ShapeDtypeStruct((length, head_count * width_v), jnp.bfloat16),
    )(offset, queries, keys_in, values_in, source_logs, target_logs, gain[:, None, :])


def position_logs(in_gate, forget_gate):
    log_decay = jax.nn.log_sigmoid(forget_gate)
    gates = lax.all_gather(jnp.stack([in_gate, log_decay]), "sp")
    inputs, decays = gates[:, 0], gates[:, 1]
    count, length = decays.shape[0], decays.shape[-1]
    upper = jnp.triu(jnp.ones((length, length), jnp.float32))
    running = jnp.einsum("ndghu,ut->ndght", decays, upper, precision=HIGHEST)
    earlier = jnp.tril(jnp.ones((count, count), jnp.float32), -1)
    before = jnp.einsum("nm,mdgh->ndgh", earlier, running[..., -1], precision=HIGHEST)
    running = running + before[..., None]
    forward_sums, backward_sums = running[:, 0], running[:, 1] - decays[:, 1]
    source = jnp.stack([inputs[:, 0] - forward_sums, inputs[:, 1] + backward_sums])
    source = source.transpose(2, 3, 0, 1, 4).reshape(
        source.shape[2], source.shape[3], 2, count * length
    )
    mine = lax.axis_index("sp")
    target = jnp.stack(
        [
            lax.dynamic_index_in_dim(forward_sums, mine, 0, keepdims=False),
            -lax.dynamic_index_in_dim(backward_sums, mine, 0, keepdims=False),
        ],
        axis=-1,
    )
    return source, target


def local(
    query_a,
    key_a,
    value_a,
    query_b,
    key_b,
    value_b,
    in_gate,
    forget_gate,
    head_gain_a,
    head_gain_b,
    out_weight_a,
    out_weight_b,
    residual,
    norm_gain,
    routes,
    route_weights,
    expert_gate,
    expert_up,
    expert_down,
):
    source_logs, target_logs = position_logs(in_gate, forget_gate)
    offset = (lax.axis_index("sp") * query_a.shape[0]).astype(jnp.int32).reshape(1)
    gathered = [
        lax.all_gather(tensor, "sp", axis=0, tiled=True)
        for tensor in (key_b, value_b, key_a, value_a)
    ]
    heads_b = group_heads(
        offset, query_b, gathered[0], gathered[1], source_logs[1], target_logs[1], head_gain_b
    )
    heads_a = group_heads(
        offset, query_a, gathered[2], gathered[3], source_logs[0], target_logs[0], head_gain_a
    )
    first_term = jnp.einsum("se,ec->cs", heads_a, out_weight_a, preferred_element_type=jnp.float32)
    mix = lax.psum_scatter(
        (
            first_term
            + jnp.einsum("se,ec->cs", heads_b, out_weight_b, preferred_element_type=jnp.float32)
        ).astype(jnp.bfloat16),
        "tp",
        scatter_dimension=0,
        tiled=True,
    ).astype(jnp.float32)
    updated = residual.astype(jnp.float32) + mix
    squares = lax.psum(jnp.sum(updated * updated, axis=0), "tp")
    whole_width = residual.shape[0] * lax.axis_size("tp")
    normed = (
        updated * lax.rsqrt(squares / whole_width + EPSILON)[None, :] * norm_gain[:, None]
    ).astype(jnp.bfloat16)
    token_count = routes.shape[0]
    top_count = routes.shape[1]
    expert_count = lax.axis_size("sp") * expert_gate.shape[0]
    slot_count = 2 * token_count * top_count // expert_count
    flat_routes = routes.reshape(-1)
    hits = (flat_routes[:, None] == jnp.arange(expert_count, dtype=jnp.int32)[None, :]).astype(
        jnp.int32
    )
    ranks = jnp.sum((jnp.cumsum(hits, axis=0) - 1) * hits, axis=1)
    targets = (flat_routes * slot_count + ranks).reshape(token_count, top_count)
    slot_ids = jnp.arange(expert_count * slot_count, dtype=jnp.int32)[:, None]
    selectors = [
        (slot_ids == targets[None, :, ordering_index]).astype(jnp.bfloat16)
        for ordering_index in range(top_count)
    ]
    dispatch = selectors[0]
    ordering_index = 1
    dispatch = dispatch + selectors[ordering_index]
    buffer = jnp.einsum("ps,ds->pd", dispatch, normed, preferred_element_type=jnp.float32)
    buffer = buffer.astype(jnp.bfloat16).reshape(expert_count, slot_count, -1)
    arrived = lax.all_to_all(buffer, "sp", split_axis=0, concat_axis=0, tiled=True)
    piece = lax.all_gather(arrived, "tp", axis=2, tiled=True)
    flat_rows = piece.reshape(-1, piece.shape[-1])
    gate_rows = expert_gate[0]
    up_rows = expert_up[0]
    gate = jnp.dot(flat_rows, gate_rows, preferred_element_type=jnp.float32)
    upward = jnp.dot(flat_rows, up_rows, preferred_element_type=jnp.float32)
    hidden = (
        (jax.nn.silu(gate) * upward)
        .astype(jnp.bfloat16)
        .reshape(arrived.shape[0], arrived.shape[1], -1)
    )
    sources = hidden.shape[0]
    hidden_rows = hidden.reshape(-1, hidden.shape[-1])
    columns = expert_down[0]
    summed = lax.psum_scatter(
        jnp.einsum("rf,fc->cr", hidden_rows, columns, preferred_element_type=jnp.float32).astype(
            jnp.bfloat16
        ),
        "tp",
        scatter_dimension=0,
        tiled=True,
    ).astype(jnp.float32)
    outgoing = summed.astype(jnp.bfloat16).reshape(summed.shape[0], sources, slot_count)
    returned = lax.all_to_all(outgoing, "sp", split_axis=1, concat_axis=1, tiled=True)
    returned = returned.reshape(returned.shape[0], -1)
    combined = updated
    for ordering_index in range(top_count):
        picked = jnp.dot(returned, selectors[ordering_index], preferred_element_type=jnp.float32)
        combined = combined + route_weights[:, ordering_index][None, :] * picked
    return combined.astype(jnp.bfloat16)


def solution(mesh):
    placed = (
        P("sp", "tp"),
        P("sp", "tp"),
        P("sp", "tp"),
        P("sp", "tp"),
        P("sp", "tp"),
        P("sp", "tp"),
        P(None, None, "tp", "sp"),
        P(None, None, "tp", "sp"),
        P("tp", None),
        P("tp", None),
        P("tp", None),
        P("tp", None),
        P("tp", "sp"),
        P("tp"),
        P("sp", None),
        P("sp", None),
        P("sp", None, "tp"),
        P("sp", None, "tp"),
        P("sp", "tp", None),
    )
    return jax.shard_map(
        local, mesh=mesh, in_specs=placed, out_specs=P("tp", "sp"), check_vma=False
    )
```

time: 501 us -> 341 us (0.68)
  waiting for transfers between devices: 83.8 us -> 219 us
  other arithmetic: 131 us -> 4.33 us
  blocking collectives: 160 us -> 58 us
  local copies, waits for them, and re-layouts: 63 us -> 4.38 us
  matrix products: 36.8 us -> 23.7 us
  Pallas kernels: 0 us -> 11.1 us
    all_gather x4, waiting for transfers between devices: 0.01 us -> 132 us  [local(): lax.all_gather(tensor, 'sp', axis=0, tiled=True)]
    select_n x70 -> x0, other arithmetic: 91.2 us -> none  [turn(): jnp.where(position < mine, new, old)]
    all_gather x4 -> x1, blocking collectives: 110 us -> 32.5 us  [position_logs(): gates = lax.all_gather(jnp.stack([in_gate, log_decay]), 'sp')]
    rev x20 -> x0, local copies, waits for them, and re-layouts: 27.1 us -> none  [the longest x8 15.5 us: carried_in(): pieces = jax.tree.map(lambda part: part[::-1], pieces)]
    unnamed x1 -> x0, blocking collectives: 24.2 us -> none
    exp x31 -> x0, other arithmetic: 20.2 us -> none  [the longest x28 19.3 us: merge_group(): scale_early = jnp.exp(shifted - merged_top)]
    unnamed x121 -> x18, local copies, waits for them, and re-layouts: 19.5 us -> 0.27 us
    dot_general x22 -> x3, matrix products: 17.9 us -> 4.59 us  [the longest x1 3.02 us: local(): jnp.einsum('se,ec->cs', heads_a, out_weight_a, preferred_element_type=jnp...]
  transfers between devices with their start and end apart: 8 -> 8, of which waited for: 4 -> 8; matrix products, arithmetic and copies ran while one was open for 27% -> 2% of each run, Pallas kernels for 0% -> 2%
where the time goes in v1:
time: 341 us; the launch traced here: 340 us
  waiting for transfers between devices  219 us (64%)
  blocking collectives  58 us (17%)
  matrix products  23.7 us (7%)
  between operations  13.8 us (4%)
  Pallas kernels  11.1 us (3%)
  starting transfers between devices  5.75 us (2%)
  local copies, waits for them, and re-layouts  4.38 us (1%)
  other arithmetic  4.33 us (1%)
    all_gather x4, waiting for transfers between devices, local(): lax.all_gather(tensor, 'sp', axis=0, tiled=True)  132 us
    all_gather x1, blocking collectives, position_logs(): gates = lax.all_gather(jnp.stack([in_gate, log_decay]), 'sp')  32.5 us
    reduce_scatter x1, waiting for transfers between devices, local(): lax.psum_scatter(jnp.einsum('rf,fc->cr', hidden_rows, columns, preferred_...  31.3 us
    all_gather x1, waiting for transfers between devices, local(): piece = lax.all_gather(arrived, 'tp', axis=2, tiled=True)  20.8 us
    all_to_all x1, blocking collectives, local(): lax.all_to_all(buffer, 'sp', split_axis=0, concat_axis=0, tiled=True)  19.8 us
    reduce_scatter x1, waiting for transfers between devices, local(): lax.psum_scatter((first_term + jnp.einsum('se,ec->cs', heads_b, out_weigh...  18.6 us
    all_to_all x1, waiting for transfers between devices, local(): lax.all_to_all(outgoing, 'sp', split_axis=1, concat_axis=1, tiled=True)  14.3 us
    pallas_call x2, Pallas kernels, group_heads(): pl.pallas_call(heads_kernel, grid_spec=pltpu.PrefetchScalarGridSpec(num_s...  11.1 us
  transfers between devices with their start and end apart: 8, of which 8 were waited for; matrix products, arithmetic and copies ran while one was open for 2% of the time, Pallas kernels for 2%

profile of v1, /device:TPU:0, one launch (start us, length us, event | category | flops | bytes accessed | tf_op | source)
XLA Modules:
  0.0 340.4 jit_solution(18052809126543227378)
XLA Ops:
  6.5 0.7 all-gather.11.cloned.1.call-update
  9.4 0.7 fusion.44
  10.8 32.5 %all-gather = f32[16,2,2,4,128]{4,3,2,1,0:T(4,128)S(1)} all-gather(f32[2,2,2,4,128]{4,3,2,1,0:T(4,128)S(1)} %pad_maximum_fusion.1), channel_id=2, replica_groups=mesh['sp'=8,'tp'=4] {'sp'}, dimensions={0}, use_global_device_ids=true | all-gather | bytes 147456 | tf_op jit(solution)/shard_map/all_gather | solution.py:62
  46.6 1.0 fusion.23
  47.6 5.0 %all-gather.11.cloned.1.call-done.keys_in = bf16[1024,512]{1,0:T(8,128)(2,1)} async-done(((bf16[128,512]{1,0:T(8,128)(2,1)}), bf16[1024,512]{1,0:T(8,128)(2,1)}) %all-gather.11.cloned.1.call-update) | async-done | bytes 1048592 | tf_op jit(solution)/shard_map/all_gather | solution.py:110
  52.7 41.2 %all-gather.13.cloned.1.call-done.values_in = bf16[1024,512]{1,0:T(8,128)(2,1)} async-done(((bf16[128,512]{1,0:T(8,128)(2,1)}), bf16[1024,512]{1,0:T(8,128)(2,1)}) %all-gather.13.cloned.1.call-update) | async-done | bytes 1048592 | tf_op jit(solution)/shard_map/all_gather | solution.py:110
  93.8 5.4 %shard_map.182 = bf16[128,512]{1,0:T(8,128)(2,1)} custom-call(s32[1]{0:T(128)} %bitcast.offset, bf16[128,512]{1,0:T(8,128)(2,1)} %queries.3, bf16[1024,512]{1,0:T(8,128)(2,1)} %all-gather.11.cloned.1.call-done.keys_in, bf16[1024,512]{1,0:T(8,128)(2,1)} %all-gather.13.cloned.1.call-done.values_in, f32[4,2,1024]{2,1,0:T(2,128)} %copy.108.source_logs, ...), custom_call_target="tpu_custom_call" | custom-call | tf_op jit(solution)/shard_map/pallas_call | solution.py:41
  99.2 35.8 %all-gather.7.cloned.1.call-done.keys_in = bf16[1024,512]{1,0:T(8,128)(2,1)} async-done(((bf16[128,512]{1,0:T(8,128)(2,1)}), bf16[1024,512]{1,0:T(8,128)(2,1)}) %all-gather.7.cloned.1.call-update) | async-done | bytes 1048592 | tf_op jit(solution)/shard_map/all_gather | solution.py:110
  135.0 49.8 %all-gather.9.cloned.1.call-done.values_in = bf16[1024,1024]{1,0:T(8,128)(2,1)} async-done(((bf16[128,1024]{1,0:T(8,128)(2,1)}), bf16[1024,1024]{1,0:T(8,128)(2,1)}) %all-gather.9.cloned.1.call-update) | async-done | bytes 2097168 | tf_op jit(solution)/shard_map/all_gather | solution.py:110
  184.8 5.7 %shard_map.181 = bf16[128,1024]{1,0:T(8,128)(2,1)} custom-call(s32[1]{0:T(128)} %bitcast.offset, bf16[128,512]{1,0:T(8,128)(2,1)} %queries.2, bf16[1024,512]{1,0:T(8,128)(2,1)} %all-gather.7.cloned.1.call-done.keys_in, bf16[1024,1024]{1,0:T(8,128)(2,1)} %all-gather.9.cloned.1.call-done.values_in, f32[4,2,1024]{2,1,0:T(2,128)} %copy.107.source_logs, ...), custom_call_target="tpu_custom_call" | custom-call | tf_op jit(solution)/shard_map/pallas_call | solution.py:41
  190.5 3.0 fusion.59
  193.6 1.3 fusion.13
  196.6 18.6 %reduce-scatter.3.cloned.1.call-done = bf16[512,128]{0,1:T(8,128)(2,1)} async-done(((bf16[2048,128]{0,1:T(8,128)(2,1)}), bf16[512,128]{0,1:T(8,128)(2,1)}) %reduce-scatter.3.cloned.1.call-update) | async-done | bytes 131088 | tf_op jit(solution)/shard_map/reduce_scatter | solution.py:120
  215.2 1.0 multiply_reduce_fusion
  216.3 5.8 %psum.7 = f32[128]{0:T(128)S(1)} all-reduce(f32[128]{0:T(128)S(1)} %multiply_reduce_fusion), channel_id=1, replica_groups=mesh['sp'=8,'tp'=4] {'tp'}, use_global_device_ids=true, to_apply=%region_5.6 | all-reduce | flops 128 | bytes 1024 | tf_op jit(solution)/shard_map/psum | solution.py:130
  222.0 1.3 convolution_convert_fusion
  223.3 19.8 %all_to_all.10 = bf16[8,64,512]{2,1,0:T(8,128)(2,1)} all-to-all(bf16[8,64,512]{2,1,0:T(8,128)(2,1)S(1)} %bitcast.90), channel_id=1, replica_groups=mesh['sp'=8,'tp'=4] {'sp'}, dimensions={0} | all-to-all | bytes 1048576 | tf_op jit(solution)/shard_map/all_to_all | solution.py:155
  243.2 20.8 %all-gather.15.cloned.1.call-done = bf16[8,64,2048]{2,1,0:T(8,128)(2,1)} async-done(((bf16[8,64,512]{2,1,0:T(8,128)(2,1)}), bf16[8,64,2048]{2,1,0:T(8,128)(2,1)}) %all-gather.15.cloned.1.call-update) | async-done | bytes 2097168 | tf_op jit(solution)/shard_map/all_gather | solution.py:156
  264.0 6.5 %fusion.4 = f32[512,1024]{1,0:T(8,128)} fusion(bf16[512,2048]{1,0:T(8,128)(2,1)} %bitcast.102, bf16[1,2048,1024]{2,1,0:T(8,128)(2,1)} %param.35), kind=kOutput, calls=%fused_computation.4 | convolution fusion | flops 2147483648 | bytes 8388608 | tf_op jit(solution)/shard_map/dot_general | solution.py:160
  270.5 10.6 %fusion.9 = bf16[2048,512]{0,1:T(8,128)(2,1)} fusion(bf16[1,1024,2048]{2,1,0:T(8,128)(2,1)} %param.37, f32[512,1024]{1,0:T(8,128)} %fusion.4, bf16[512,2048]{1,0:T(8,128)(2,1)} %bitcast.103, bf16[1,2048,1024]{2,1,0:T(8,128)(2,1)} %param.36), kind=kOutput, calls=%fused_computation.7 | convolution fusion | flops 4299161600 | bytes 14680064 | tf_op jit(solution)/shard_map/rf,fc->cr/dot_general | solution.py:171
  281.1 31.3 %reduce-scatter.5.cloned.1.call-done = bf16[512,512]{0,1:T(8,128)(2,1)} async-done(((bf16[2048,512]{0,1:T(8,128)(2,1)}), bf16[512,512]{0,1:T(8,128)(2,1)}) %reduce-scatter.5.cloned.1.call-update) | async-done | bytes 524304 | tf_op jit(solution)/shard_map/reduce_scatter | solution.py:170
  312.4 5.5 %all-to-all-start.1 = ((bf16[512,8,64]{0,2,1:T(8,128)(2,1)}), bf16[512,8,64]{0,2,1:T(8,128)(2,1)S(1)}, u32[]{:S(2)}, u32[]{:S(2)}) async-start(bf16[512,8,64]{0,2,1:T(8,128)(2,1)} %bitcast.91), calls=%async_computation.3 | async-start | bytes 1048576 | tf_op jit(solution)/shard_map/all_to_all | solution.py:179
  317.9 14.3 %all-to-all-done.1 = bf16[512,8,64]{0,2,1:T(8,128)(2,1)S(1)} async-done(((bf16[512,8,64]{0,2,1:T(8,128)(2,1)}), bf16[512,8,64]{0,2,1:T(8,128)(2,1)S(1)}, u32[]{:S(2)}, u32[]{:S(2)}) %all-to-all-start.1) | async-done | bytes 524320 | tf_op jit(solution)/shard_map/all_to_all | solution.py:179
  332.8 0.8 copy.103
  (67 shorter events, 8.4 us)
Async XLA Ops:
  6.5 187.0 %copy-start = (bf16[512,2048]{1,0:T(8,128)(2,1)S(1)}, bf16[512,2048]{1,0:T(8,128)(2,1)}, u32[]{:S(2)}) copy-start(bf16[512,2048]{1,0:T(8,128)(2,1)} %param.30) | copy-start | bytes 6291460
  6.5 38.9 %copy-start.5 = (f32[4,256]{1,0:T(4,128)S(1)}, f32[4,256]{1,0:T(4,128)}, u32[]{:S(2)}) copy-start(f32[4,256]{1,0:T(4,128)} %param.27) | copy-start | bytes 12292
  6.5 46.1 %all-gather.11.cloned.1.call-start = ((), (), s32[]{:S(2)}) async-start(), calls=%async_computation.6 | async-start | bytes 1179648 | tf_op jit(solution)/shard_map/all_gather | solution.py:110
  7.3 86.6 %all-gather.13.cloned.1.call-start = ((), (), s32[]{:S(2)}) async-start(), calls=%async_computation.7 | async-start | bytes 1179648 | tf_op jit(solution)/shard_map/all_gather | solution.py:110
  8.0 127.0 %all-gather.7.cloned.1.call-start = ((), (), s32[]{:S(2)}) async-start(), calls=%async_computation.4 | async-start | bytes 1179648 | tf_op jit(solution)/shard_map/all_gather | solution.py:110
  8.7 176.1 %all-gather.9.cloned.1.call-start = ((), (), s32[]{:S(2)}) async-start(), calls=%async_computation.5 | async-start | bytes 2359296 | tf_op jit(solution)/shard_map/all_gather | solution.py:110
  9.3 205.9 %reduce-scatter.3.cloned.1.call-start = ((), (), s32[]{:S(2)}) async-start(), calls=%async_computation.8 | async-start | bytes 655360 | tf_op jit(solution)/shard_map/reduce_scatter | solution.py:120
  190.5 3.0 copy-start.2
  193.5 1.4 copy-start.4
  193.5 1.8 copy-start.3
  193.5 28.5 %copy-start.6 = (f32[512]{0:T(512)S(1)}, f32[512]{0:T(512)}, u32[]{:S(2)}) copy-start(f32[512]{0:T(512)} %param.32) | copy-start | bytes 6148
  194.9 69.1 %all-gather.15.cloned.1.call-start = ((), (), s32[]{:S(2)}) async-start(), calls=%async_computation.9 | async-start | bytes 2621440 | tf_op jit(solution)/shard_map/all_gather | solution.py:156
  243.1 69.3 %reduce-scatter.5.cloned.1.call-start = ((), (), s32[]{:S(2)}) async-start(), calls=%async_computation.10 | async-start | bytes 2621440 | tf_op jit(solution)/shard_map/reduce_scatter | solution.py:170
  281.0 36.9 %copy-start.7 = (f32[128,2]{0,1:T(2,128)S(1)}, f32[128,2]{0,1:T(2,128)}, u32[]{:S(2)}) copy-start(f32[128,2]{0,1:T(2,128)} %param.34) | copy-start | bytes 3076
  281.0 51.2 %copy-start.1 = (bf16[512,128]{0,1:T(8,128)(2,1)S(1)}, bf16[512,128]{0,1:T(8,128)(2,1)}, u32[]{:S(2)}) copy-start(bf16[512,128]{0,1:T(8,128)(2,1)} %reduce-scatter.3.cloned.1.call-done) | copy-start | bytes 393220
  312.4 19.8 %all-to-all-start.1 = ((bf16[512,8,64]{0,2,1:T(8,128)(2,1)}), bf16[512,8,64]{0,2,1:T(8,128)(2,1)S(1)}, u32[]{:S(2)}, u32[]{:S(2)}) async-start(bf16[512,8,64]{0,2,1:T(8,128)(2,1)} %bitcast.91), calls=%async_computation.3 | async-start | bytes 1048576 | tf_op jit(solution)/shard_map/all_to_all | solution.py:179
Sparse Core Ops, SparseCore 0:
  9.5 43.1 all-gather.10
  54.8 38.9 all-gather.12
  96.0 38.9 all-gather.6
  137.0 47.7 all-gather.8
  195.0 20.1 reduce-scatter.2
  243.3 20.6 all-gather.14
  281.2 31.1 reduce-scatter.4
